TPU v7x, 32 devices: a whole 2x2x4 slice. The times are simulated.
32 devices in a mesh: ep: 16 (over z, x, core), tp: 2 (over y).
Axes of the slice: x: 2, y: 2, z: 4, core: 2. Of those that a mesh axis runs over, the one named last changes fastest.
Arguments:
- tokens: bfloat16 [256, 2048], P('ep'), may hold values from -6 to 6
- attn_gain: bfloat16 [2048], replicated, may hold values from 0.099609375 to 1.8984375
- query_weight: bfloat16 [2048, 1024], P('ep', 'tp'), may hold values from -0.125 to 0.125
- key_weight: bfloat16 [2048, 512], P('ep', 'tp'), may hold values from -0.125 to 0.125
- value_weight: bfloat16 [2048, 512], P('ep', 'tp'), may hold values from -0.125 to 0.125
- out_weight: bfloat16 [2048, 1024], P('ep', 'tp'), may hold values from -0.1875 to 0.1875
- head_gain: bfloat16 [1024], P('tp'), may hold values from 0.099609375 to 1.8984375
- past_keys: bfloat16 [256, 1024, 4, 128], P('ep', None, 'tp'), may hold values from -6 to 6
- past_values: bfloat16 [256, 1024, 4, 128], P('ep', None, 'tp'), may hold values from -50 to 50
- break_offset: float32 [256, 8, 1024], P('ep', 'tp'), may hold values from -12.5 to 1
- cache_lengths: int32 [256], P('ep'), may hold values from 1 to 1024, 131072 in all
- ffn_gain: bfloat16 [2048], replicated, may hold values from 0.099609375 to 1.8984375
- router_weight: bfloat16 [2048, 16], replicated, may hold values from -0.25 to 0.25
- expert_routes: int32 [256, 6], P('ep'), may hold values from 0 to 15, all different within a row; in each aligned block of 16 rows (0 to 15, 16 to 31, ...) at most 12 rows name the same one
- expert_gate: bfloat16 [16, 2048, 512], P('ep', None, 'tp'), may hold values from -0.125 to 0.125
- expert_up: bfloat16 [16, 2048, 512], P('ep', None, 'tp'), may hold values from -0.125 to 0.125
- expert_down: bfloat16 [16, 512, 2048], P('ep', 'tp'), may hold values from -0.25 to 0.25
- shared_gate: bfloat16 [2048, 512], P(None, 'tp'), may hold values from -0.125 to 0.125
- shared_up: bfloat16 [2048, 512], P(None, 'tp'), may hold values from -0.125 to 0.125
- shared_down: bfloat16 [512, 2048], P('tp'), may hold values from -0.25 to 0.25
Outputs:
- mixed: bfloat16 [256, 2048], P('ep', 'tp')
- fresh_keys: bfloat16 [256, 512], P('ep', 'tp')
- fresh_values: bfloat16 [256, 512], P('ep', 'tp')
Inputs may be any that keep to these rules, and one draw needn't show every extreme that they name: `cache_lengths`: the lengths add up to half of 262144, and some sequence has length 1024. `expert_routes`: each row names 6 different experts. Among the rows of one device no expert is named more than 12 times, and 12 is reached in some device's rows.
All inputs are finite; a program needn't handle non-finite values. No bound on the sum of `cache_lengths` on one device may be relied on, other than what follows from the above.
Results may differ from a plain program's by a relative error of at most 0.0095.
Values may be sent and summed in bfloat16 or wider, within the bound.
A program may use at most 64 MiB of HBM per device.

v0:
```python
import jax
import jax.numpy as jnp
from jax import lax
from jax.sharding import PartitionSpec as P

HQ = 8
HD = 128


epsilon = 1e-06
routed_scale = 2.5


def root_norm(values, gain):
    data = values.astype(jnp.float32)
    factor = lax.rsqrt(jnp.mean(data * data, axis=-1, keepdims=True) + epsilon)
    return (data * factor * gain.astype(jnp.float32)).astype(jnp.bfloat16)


def stick_attend(queries, key_cache, value_cache, offsets, lengths):
    seq_count, positions, key_heads, head_size = key_cache.shape
    heads_local = offsets.shape[1]
    group_size = heads_local // key_heads
    grouped = queries.reshape(seq_count, key_heads, group_size, head_size)
    scores = jnp.einsum("bgrd,blgd->bgrl", grouped, key_cache, preferred_element_type=jnp.float32)
    logits = scores.reshape(seq_count, heads_local, positions) * head_size ** (-0.5) + offsets
    places = lax.broadcasted_iota(jnp.int32, (1, 1, positions), 2)
    usable = places < lengths[:, None, None]
    keep_log = jnp.where(usable, jax.nn.log_sigmoid(-logits), 0.0)
    after_sum = jnp.sum(keep_log, axis=-1, keepdims=True) - jnp.cumsum(keep_log, axis=-1)
    sticks = jnp.where(usable, jnp.exp(jax.nn.log_sigmoid(logits) + after_sum), 0.0).astype(
        jnp.bfloat16
    )
    sticks = sticks.reshape(seq_count, key_heads, group_size, positions)
    outputs = jnp.einsum("bgrl,blgd->bgrd", sticks, value_cache, preferred_element_type=jnp.float32)
    return outputs.reshape(seq_count, heads_local * head_size)


def body(
    tokens,
    attn_gain,
    query_weight,
    key_weight,
    value_weight,
    out_weight,
    head_gain,
    past_keys,
    past_values,
    break_offset,
    cache_lengths,
    ffn_gain,
    router_weight,
    expert_routes,
    expert_gate,
    expert_up,
    expert_down,
    shared_gate,
    shared_up,
    shared_down,
):
    seq_count = tokens.shape[0]
    model_width = tokens.shape[1]
    query_cols = query_weight.shape[1]
    key_cols = key_weight.shape[1]
    normed = root_norm(tokens, attn_gain)
    features = lax.all_to_all(normed, "ep", split_axis=1, concat_axis=0, tiled=True)
    joined = jnp.concatenate([query_weight, key_weight, value_weight], axis=1)
    projected = lax.psum_scatter(
        jnp.dot(features, joined, preferred_element_type=jnp.float32),
        "ep",
        scatter_dimension=0,
        tiled=True,
    )
    queries = projected[:, :query_cols].astype(jnp.bfloat16)
    fresh_keys = projected[:, query_cols : query_cols + key_cols].astype(jnp.bfloat16)
    fresh_values = projected[:, query_cols + key_cols :].astype(jnp.bfloat16)
    experts = router_weight.shape[1]
    top_count = expert_routes.shape[1]
    capacity = max(2, min(seq_count, (2 * seq_count * top_count + experts - 1) // experts))
    local_experts = expert_gate.shape[0]
    column_width = model_width // lax.axis_size("tp")
    block_count = 1
    block_rows = seq_count // block_count
    heads_out = stick_attend(queries, past_keys, past_values, break_offset, cache_lengths)
    scaled = (heads_out * head_gain.astype(jnp.float32)).astype(jnp.bfloat16)
    square_sum = jnp.sum(heads_out * heads_out, axis=-1)
    feature_cols = jnp.einsum(
        "nc,dc->nd",
        lax.all_gather(scaled, "ep", axis=0, tiled=True),
        out_weight,
        preferred_element_type=jnp.float32,
    ).astype(jnp.bfloat16)
    partial_value = lax.all_to_all(feature_cols, "ep", split_axis=0, concat_axis=1, tiled=True)
    all_parts = lax.all_gather(partial_value[None], "tp", axis=0, tiled=True)
    head_total = jnp.sum(all_parts.astype(jnp.float32), axis=0)
    square_total = lax.psum(square_sum, "tp")
    attention = head_total * lax.rsqrt(square_total[:, None] / (HQ * HD) + epsilon)
    residual = (tokens.astype(jnp.float32) + attention).astype(jnp.bfloat16)
    normed_ffn = root_norm(residual, ffn_gain)
    router_prob = jax.nn.sigmoid(
        jnp.dot(normed_ffn, router_weight, preferred_element_type=jnp.float32)
    )
    chosen = expert_routes[:, :, None] == lax.broadcasted_iota(jnp.int32, (1, 1, experts), 2)
    picked = jnp.sum(jnp.where(chosen, router_prob[:, None, :], 0.0), axis=-1)
    route_weight = routed_scale * picked / jnp.sum(picked, axis=-1, keepdims=True)
    flat_hot = chosen.reshape(block_rows * top_count, experts).astype(jnp.int32)
    earlier = jnp.cumsum(flat_hot, axis=0) - flat_hot
    slot_index = jnp.sum(earlier * flat_hot, axis=-1).reshape(block_rows, top_count)
    slot_hot = (
        slot_index[:, :, None] == lax.broadcasted_iota(jnp.int32, (1, 1, capacity), 2)
    ).astype(jnp.float32)
    expert_hot = chosen.astype(jnp.float32)
    dispatch = jnp.einsum("ske,skc->ecs", expert_hot, slot_hot)
    weighted = jnp.sum(
        route_weight[:, :, None, None] * expert_hot[:, :, :, None] * slot_hot[:, :, None, :], axis=1
    )
    outbound = jnp.einsum(
        "ecs,sd->ecd", dispatch.astype(jnp.bfloat16), normed_ffn, preferred_element_type=jnp.float32
    ).astype(jnp.bfloat16)
    arrived = lax.all_to_all(outbound, "ep", split_axis=0, concat_axis=0, tiled=True)
    item_count = arrived.shape[1]
    sources = arrived.shape[0] // local_experts
    grouped = arrived.reshape(sources, local_experts, item_count, model_width)
    gate_part = jnp.einsum(
        "sxcd,xdf->sxcf", grouped, expert_gate, preferred_element_type=jnp.float32
    )
    up_part = jnp.einsum("sxcd,xdf->sxcf", grouped, expert_up, preferred_element_type=jnp.float32)
    hidden = (jax.nn.silu(gate_part) * up_part).astype(jnp.bfloat16)
    down_part = jnp.einsum(
        "sxcf,xfd->sxcd", hidden, expert_down, preferred_element_type=jnp.float32
    )
    expert_part = down_part.astype(jnp.bfloat16).reshape(arrived.shape)
    shared_hidden = (
        jax.nn.silu(jnp.dot(normed_ffn, shared_gate, preferred_element_type=jnp.float32))
        * jnp.dot(normed_ffn, shared_up, preferred_element_type=jnp.float32)
    ).astype(jnp.bfloat16)
    shared_part = jnp.dot(shared_hidden, shared_down, preferred_element_type=jnp.float32).astype(
        jnp.bfloat16
    )
    expert_pieces = lax.all_to_all(expert_part[None], "tp", split_axis=3, concat_axis=0, tiled=True)
    shared_pieces = lax.all_to_all(
        shared_part[None, None], "tp", split_axis=3, concat_axis=0, tiled=True
    )
    expert_total = jnp.sum(expert_pieces.astype(jnp.float32), axis=0)
    shared_total = jnp.sum(shared_pieces.astype(jnp.float32), axis=0)
    returned = lax.all_to_all(
        expert_total.astype(jnp.bfloat16), "ep", split_axis=0, concat_axis=0, tiled=True
    )
    routed = jnp.einsum(
        "sec,ecd->sd", weighted, returned.astype(jnp.float32), precision=lax.Precision.HIGHEST
    )
    own_cols = lax.dynamic_slice_in_dim(
        residual, lax.axis_index("tp") * column_width, column_width, 1
    )
    results = (own_cols.astype(jnp.float32) + routed + shared_total[0]).astype(jnp.bfloat16)
    return (results, fresh_keys, fresh_values)


def solution(mesh):
    placed = (
        P("ep", None),
        P(),
        P("ep", "tp"),
        P("ep", "tp"),
        P("ep", "tp"),
        P("ep", "tp"),
        P("tp"),
        P("ep", None, "tp", None),
        P("ep", None, "tp", None),
        P("ep", "tp", None),
        P("ep"),
        P(),
        P(),
        P("ep", None),
        P("ep", None, "tp"),
        P("ep", None, "tp"),
        P("ep", "tp", None),
        P(None, "tp"),
        P(None, "tp"),
        P("tp", None),
    )
    return jax.shard_map(
        body,
        mesh=mesh,
        in_specs=placed,
        out_specs=(P("ep", "tp"), P("ep", "tp"), P("ep", "tp")),
        check_vma=False,
    )
```

profile of v0, /device:TPU:0, one launch (start us, length us, event | category | flops | bytes accessed | tf_op | source)
XLA Modules:
  0.0 279.9 jit_solution(1717214393868574309)
XLA Ops:
  9.9 14.1 %all_to_all.66 = bf16[16,16,128]{2,0,1:T(8,128)(2,1)S(1)} all-to-all(bf16[16,16,128]{2,0,1:T(8,128)(2,1)S(1)} %copy_bitcast_fusion), channel_id=1, replica_groups=mesh['ep'=16,'tp'=2] {'ep'}, dimensions={1} | all-to-all | bytes 131072 | tf_op jit(solution)/shard_map/all_to_all | solution.py:66
  24.0 2.2 fusion.33
  30.7 50.7 %reduce-scatter.2.cloned.1.call-done = f32[16,1024]{1,0:T(8,128)} async-done(((f32[256,1024]{1,0:T(8,128)}), f32[16,1024]{1,0:T(8,128)}) %reduce-scatter.2.cloned.1.call-update) | async-done | bytes 65552 | tf_op jit(solution)/shard_map/reduce_scatter | solution.py:68
  82.3 5.6 %fusion.19 = f32[16,2,2,1024]{3,2,1,0:T(2,128)S(1)} fusion(bf16[16,2,2,128]{3,2,1,0:T(2,128)(2,1)S(1)} %reshape.155, bf16[16,1024,2,128]{3,2,1,0:T(2,128)(2,1)} %param.27), kind=kOutput, calls=%fused_computation.27 | convolution fusion | flops 16842752 | bytes 8667136 | tf_op jit(solution)/shard_map/bgrd,blgd->bgrl/dot_general | solution.py:25
  88.7 18.0 %reduce-window.6 = f32[16,4,8,128]{3,2,1,0:T(8,128)S(1)} reduce-window(f32[16,4,8,128]{3,2,1,0:T(8,128)S(1)} %reshape.156, f32[]{:T(128)} %constant.20.clone.1), window={size=1x1x1x128 pad=0_0x0_0x0_0x127_0}, to_apply=%region_3.4 | reduce-window | flops 8323072 | bytes 524292 | tf_op jit(solution)/shard_map/reduce-window
  108.1 4.9 %multiply_reduce_fusion.1 = (f32[16]{0:T(128)S(1)}, f32[16,2,2,128]{3,2,1,0:T(2,128)S(1)}) fusion(bf16[16,2,2,1024]{3,2,1,0:T(2,128)(2,1)S(1)} %reshape.158, bf16[16,1024,2,128]{3,2,1,0:T(2,128)(2,1)} %param.28), kind=kOutput, calls=%fused_computation.81 | convolution fusion | flops 16793584 | bytes 8552512 | tf_op jit(solution)/shard_map/bgrl,blgd->bgrd/dot_general | solution.py:35
  113.0 20.1 %all_gather.6 = bf16[256,512]{1,0:T(8,128)(2,1)S(1)} all-gather(bf16[16,512]{1,0:T(8,128)(2,1)S(1)} %multiply_convert_fusion), channel_id=1, replica_groups=mesh['ep'=16,'tp'=2] {'ep'}, dimensions={0}, use_global_device_ids=true | all-gather | bytes 278528 | tf_op jit(solution)/shard_map/all_gather | solution.py:89
  134.0 3.5 %all-to-all-start.1 = ((bf16[16,16,128]{2,1,0:T(8,128)(2,1)}), bf16[16,16,128]{2,1,0:T(8,128)(2,1)S(1)}, u32[]{:S(2)}, u32[]{:S(2)}) async-start(bf16[16,16,128]{2,1,0:T(8,128)(2,1)} %bitcast.3), calls=%async_computation.2 | async-start | bytes 131072 | tf_op jit(solution)/shard_map/all_to_all | solution.py:93
  137.5 4.9 %psum.7 = f32[16]{0:T(128)S(1)} all-reduce(f32[16]{0:T(128)S(1)} %get-tuple-element.9), channel_id=1, replica_groups=mesh['ep'=16,'tp'=2] {'tp'}, use_global_device_ids=true, to_apply=%region_7.8 | all-reduce | flops 16 | bytes 128 | tf_op jit(solution)/shard_map/psum | solution.py:96
  142.5 1.9 all-to-all-done.1
  144.4 4.9 %all_gather.7 = bf16[2,16,2048]{2,1,0:T(8,128)(2,1)S(1)} all-gather(bf16[1,16,2048]{2,1,0:T(8,128)(2,1)S(1)} %broadcast_in_dim.31), channel_id=1, replica_groups=mesh['ep'=16,'tp'=2] {'tp'}, dimensions={0}, use_global_device_ids=true | all-gather | bytes 196608 | tf_op jit(solution)/shard_map/all_gather | solution.py:94
  149.6 1.3 convolution_convert_fusion.1
  150.9 1.4 copy.77
  152.3 4.0 %all-to-all-start.2 = ((bf16[16,12,2048]{2,1,0:T(8,128)(2,1)}), bf16[16,12,2048]{2,1,0:T(8,128)(2,1)S(1)}, u32[]{:S(2)}, u32[]{:S(2)}) async-start(bf16[16,12,2048]{2,1,0:T(8,128)(2,1)} %copy.77), calls=%async_computation.3 | async-start | bytes 2097152 | tf_op jit(solution)/shard_map/all_to_all | solution.py:120
  157.5 21.8 %all-to-all-done.2 = bf16[16,12,2048]{2,1,0:T(8,128)(2,1)S(1)} async-done(((bf16[16,12,2048]{2,1,0:T(8,128)(2,1)}), bf16[16,12,2048]{2,1,0:T(8,128)(2,1)S(1)}, u32[]{:S(2)}, u32[]{:S(2)}) %all-to-all-start.2) | async-done | bytes 786464 | tf_op jit(solution)/shard_map/all_to_all | solution.py:120
  179.2 1.7 convolution_bitcast_fusion.1
  180.9 1.7 fusion.14
  183.0 8.5 %copy.79 = bf16[1,16,12,2048]{1,2,0,3:T(8,128)(2,1)} copy(bf16[1,16,12,2048]{3,1,2,0:T(8,128)(2,1)S(1)} %fusion.5) | data formatting | bytes 1572864 | tf_op jit(solution)/shard_map/broadcast_in_dim;reshape | solution.py:140
  191.5 9.6 %reshape.172 = bf16[2,2,98304]{2,1,0:T(2,128)(2,1)} reshape(bf16[2048,1,12,16]{3,2,1,0:T(8,128)(2,1)} %bitcast.89) | data formatting | bytes 1572864
  201.1 3.5 %all-to-all-start.3 = ((bf16[2,2,98304]{2,1,0:T(2,128)(2,1)}), bf16[2,2,98304]{2,1,0:T(2,128)(2,1)S(1)}, u32[]{:S(2)}, u32[]{:S(2)}) async-start(bf16[2,2,98304]{2,1,0:T(2,128)(2,1)} %reshape.172), calls=%async_computation.4 | async-start | bytes 1572864 | tf_op jit(solution)/shard_map/all_to_all | solution.py:140
  204.6 2.0 fusion.6
  207.9 11.5 %reduce.10 = bf16[2048,16]{1,0:T(8,128)(2,1)S(1)} reduce(bf16[2048,1,1,16]{3,2,1,0:T(2,128)(2,1)S(1)} %bitcast.90, bf16[]{:T(256)} %broadcast.123), dimensions={1,2}, to_apply=%bitcast.69.reduce_sub_computation | reduce | bytes 131074
  219.4 1.2 reshape.170
  220.6 1.0 fusion.25
  221.6 3.5 %all-to-all-start.5 = ((bf16[2,2,8192]{2,1,0:T(2,128)(2,1)}), bf16[2,2,8192]{2,1,0:T(2,128)(2,1)S(1)}, u32[]{:S(2)}, u32[]{:S(2)}) async-start(bf16[2,2,8192]{2,1,0:T(2,128)(2,1)} %reshape.170), calls=%async_computation.6 | async-start | bytes 131072 | tf_op jit(solution)/shard_map/all_to_all | solution.py:141
  225.5 9.8 %reshape.173 = bf16[2048,1,12,16]{3,2,1,0:T(8,128)(2,1)} reshape(bf16[2,2,98304]{2,1,0:T(2,128)(2,1)S(1)} %all-to-all-done.3) | data formatting | bytes 1572864
  235.3 8.7 %reduce_sum.111 = bf16[16,12,1024]{0,1,2:T(8,128)(2,1)} reduce(bf16[16,12,2,1024]{0,1,3,2:T(8,128)(2,1)} %bitcast.88, bf16[]{:T(256)} %constant.44.clone.1), dimensions={2}, to_apply=%region_14.15 | reduce | flops 196608 | bytes 1179650 | tf_op jit(solution)/shard_map/reduce_sum | solution.py:144
  244.0 5.6 %copy.80 = bf16[16,12,1024]{2,1,0:T(8,128)(2,1)} copy(bf16[16,12,1024]{0,1,2:T(8,128)(2,1)} %reduce_sum.111) | data formatting | bytes 786432 | tf_op jit(solution)/shard_map/reduce_sum | solution.py:144
  249.6 6.8 %all-to-all-start.4 = ((bf16[16,12,1024]{2,1,0:T(8,128)(2,1)}), bf16[16,12,1024]{2,1,0:T(8,128)(2,1)}, u32[]{:S(2)}, u32[]{:S(2)}) async-start(bf16[16,12,1024]{2,1,0:T(8,128)(2,1)} %copy.80), calls=%async_computation.5 | async-start | bytes 1048576 | tf_op jit(solution)/shard_map/all_to_all | solution.py:146
  257.7 1.1 bitcast_convert_fusion
  259.1 11.7 %all-to-all-done.4 = bf16[16,12,1024]{2,1,0:T(8,128)(2,1)} async-done(((bf16[16,12,1024]{2,1,0:T(8,128)(2,1)}), bf16[16,12,1024]{2,1,0:T(8,128)(2,1)}, u32[]{:S(2)}, u32[]{:S(2)}) %all-to-all-start.4) | async-done | bytes 393248 | tf_op jit(solution)/shard_map/all_to_all | solution.py:146
  270.8 2.3 fusion.18
  (69 shorter events, 15.7 us)
Async XLA Ops:
  7.2 175.4 %copy-start = (bf16[1,256,2048]{2,1,0:T(8,128)(2,1)S(1)}, bf16[1,256,2048]{2,1,0:T(8,128)(2,1)}, u32[]{:S(2)}) copy-start(bf16[1,256,2048]{2,1,0:T(8,128)(2,1)} %param.36) | copy-start | bytes 3145732
  7.2 81.0 %copy-start.4 = (f32[16,4,1024]{2,1,0:T(4,128)S(1)}, f32[16,4,1024]{2,1,0:T(4,128)}, u32[]{:S(2)}) copy-start(f32[16,4,1024]{2,1,0:T(4,128)} %param.29) | copy-start | bytes 786436
  7.2 74.2 %reduce-scatter.2.cloned.1.call-start = ((), (), s32[]{:S(2)}) async-start(), calls=%async_computation.7 | async-start | bytes 1114112 | tf_op jit(solution)/shard_map/reduce_scatter | solution.py:68
  87.9 45.2 %copy-start.5 = (bf16[128,512]{1,0:T(8,128)(2,1)S(1)}, bf16[128,512]{1,0:T(8,128)(2,1)}, u32[]{:S(2)}) copy-start(bf16[128,512]{1,0:T(8,128)(2,1)} %param.25) | copy-start | bytes 393220
  88.2 61.2 %copy-start.3 = (bf16[16,2048]{1,0:T(8,128)(2,1)S(1)}, bf16[16,2048]{1,0:T(8,128)(2,1)}, u32[]{:S(2)}) copy-start(bf16[16,2048]{1,0:T(8,128)(2,1)} %param.20) | copy-start | bytes 196612
  108.0 49.2 %copy-start.2 = (bf16[2048,256]{1,0:T(8,128)(2,1)S(1)}, bf16[2048,256]{1,0:T(8,128)(2,1)}, u32[]{:S(2)}) copy-start(bf16[2048,256]{1,0:T(8,128)(2,1)} %param.37) | copy-start | bytes 3145732
  134.0 10.4 %all-to-all-start.1 = ((bf16[16,16,128]{2,1,0:T(8,128)(2,1)}), bf16[16,16,128]{2,1,0:T(8,128)(2,1)S(1)}, u32[]{:S(2)}, u32[]{:S(2)}) async-start(bf16[16,16,128]{2,1,0:T(8,128)(2,1)} %bitcast.3), calls=%async_computation.2 | async-start | bytes 131072 | tf_op jit(solution)/shard_map/all_to_all | solution.py:93
  152.3 26.9 %all-to-all-start.2 = ((bf16[16,12,2048]{2,1,0:T(8,128)(2,1)}), bf16[16,12,2048]{2,1,0:T(8,128)(2,1)S(1)}, u32[]{:S(2)}, u32[]{:S(2)}) async-start(bf16[16,12,2048]{2,1,0:T(8,128)(2,1)} %copy.77), calls=%async_computation.3 | async-start | bytes 2097152 | tf_op jit(solution)/shard_map/all_to_all | solution.py:120
  191.5 13.1 %copy-start.1 = (bf16[256,2048]{1,0:T(8,128)(2,1)S(1)}, bf16[256,2048]{1,0:T(8,128)(2,1)}, u32[]{:S(2)}) copy-start(bf16[256,2048]{1,0:T(8,128)(2,1)} %param.39) | copy-start | bytes 3145732
  201.1 20.6 %all-to-all-start.3 = ((bf16[2,2,98304]{2,1,0:T(2,128)(2,1)}), bf16[2,2,98304]{2,1,0:T(2,128)(2,1)S(1)}, u32[]{:S(2)}, u32[]{:S(2)}) async-start(bf16[2,2,98304]{2,1,0:T(2,128)(2,1)} %reshape.172), calls=%async_computation.4 | async-start | bytes 1572864 | tf_op jit(solution)/shard_map/all_to_all | solution.py:140
  221.6 28.0 %all-to-all-start.5 = ((bf16[2,2,8192]{2,1,0:T(2,128)(2,1)}), bf16[2,2,8192]{2,1,0:T(2,128)(2,1)S(1)}, u32[]{:S(2)}, u32[]{:S(2)}) async-start(bf16[2,2,8192]{2,1,0:T(2,128)(2,1)} %reshape.170), calls=%async_computation.6 | async-start | bytes 131072 | tf_op jit(solution)/shard_map/all_to_all | solution.py:141
  249.6 21.2 %all-to-all-start.4 = ((bf16[16,12,1024]{2,1,0:T(8,128)(2,1)}), bf16[16,12,1024]{2,1,0:T(8,128)(2,1)}, u32[]{:S(2)}, u32[]{:S(2)}) async-start(bf16[16,12,1024]{2,1,0:T(8,128)(2,1)} %copy.80), calls=%async_computation.5 | async-start | bytes 1048576 | tf_op jit(solution)/shard_map/all_to_all | solution.py:146
Sparse Core Ops, SparseCore 0:
  26.4 54.9 reduce-scatter.1
where the time goes:
time: 281 us; the launch traced here: 280 us
  waiting for transfers between devices  86.1 us (31%)
  other arithmetic  47.6 us (17%)
  blocking collectives  44.1 us (16%)
  local copies, waits for them, and re-layouts  41.1 us (15%)
  matrix products  25.1 us (9%)
  starting transfers between devices  21.5 us (8%)
  between operations  14.4 us (5%)
    reduce_scatter x1, waiting for transfers between devices, body(): lax.psum_scatter(jnp.dot(features, joined, preferred_element_type=jnp.flo...  50.7 us
    unnamed x18, local copies, waits for them, and re-layouts  22.6 us
    all_to_all x1, waiting for transfers between devices, body(): lax.all_to_all(outbound, 'ep', split_axis=0, concat_axis=0, tiled=True)  21.8 us
    all_gather x1, blocking collectives, body(): lax.all_gather(scaled, 'ep', axis=0, tiled=True)  20.1 us
    another operation x4, other arithmetic  19 us
    all_to_all x1, blocking collectives, body(): lax.all_to_all(normed, 'ep', split_axis=1, concat_axis=0, tiled=True)  14.1 us
    all_to_all x1, waiting for transfers between devices, body(): lax.all_to_all(expert_total.astype(jnp.bfloat16), 'ep', split_axis=0, con...  11.7 us
    unnamed x1, other arithmetic  11.5 us
  transfers between devices with their start and end apart: 6, of which 4 were waited for; matrix products, arithmetic and copies ran while one was open for 18% of the time, Pallas kernels for 0%

commit v1 on v0

--- a/solution.py
+++ b/solution.py
@@ -1,6 +1,10 @@
+import functools
+
 import jax
 import jax.numpy as jnp
 from jax import lax
+from jax.experimental import pallas as pl
+from jax.experimental.pallas import tpu as pltpu
 from jax.sharding import PartitionSpec as P
 
 HQ = 8
@@ -156,6 +160,465 @@
     return (results, fresh_keys, fresh_values)
 
 
+MESH = pl.DeviceIdType.MESH
+F32 = jnp.float32
+BF16 = jnp.bfloat16
+
+
+def fits(ep_count, tp_count, arrays):
+    tokens, query_weight, past_keys, break_offset = arrays[0], arrays[2], arrays[7], arrays[9]
+    return (
+        ep_count == 16
+        and tp_count == 2
+        and query_weight.shape[0] % 128 == 0
+        and past_keys.shape[2] == 2
+        and break_offset.shape[1] == 4
+        and past_keys.shape[3] == 128
+        and past_keys.shape[1] % 128 == 0
+        and tokens.shape[0] == 16
+        and arrays[14].shape[0] == 1
+        and arrays[12].shape[1] <= 64
+    )
+
+
+def fused_kernel(
+    tokens_h, gains_v, wq_h, wk_h, wv_h, wo_h, keys_h, values_h, offset_h, lengths_h,
+    router_h, routes_h, eg_h, eu_h, ed_h, sg_h, su_h, sd_h,
+    mixed_o, fk_o, fv_o,
+    tok, w_qkv, w_o, kc, vc, off, lens, rt, routes, e1, e2, s1, s2,
+    nrm, tok_in, q_send, q_in, kv_send, kv_in, q4, tmat, oint, p4, ho,
+    sc_in, f_send, f_in, f_in2, sq_send, sq_in, nf_in, resid, d_send, y_in, x_send, x_in, z_send, z_in, hilo, ones, sums,
+    loc, core_s, core_r, tok_s, tok_r, qs, qr, kvs, kvr, scs, scr, fs, fr, gs, gr, sqs, sqr,
+    nzs, nzr, nxs, nxr, ys, yr, xs, xr, zs, zr,
+):
+    e = lax.axis_index("ep")
+    t = lax.axis_index("tp")
+    c = lax.rem(e, 2)
+    p = e // 2
+    x = lax.rem(p, 2)
+    z = p // 2
+    seqs = tok.shape[0]
+    width = tok.shape[1]
+    pair = width // 8
+    half = width // 2
+    span = kc.shape[1]
+    experts = router_h.shape[0]
+
+    def ep_id(peer):
+        return {"ep": peer * 2 + c}
+
+    core_id = {"ep": p * 2 + (1 - c)}
+    tp_id = {"tp": 1 - t}
+
+    def remote(src, dst, ssem, rsem, device):
+        return pltpu.make_async_remote_copy(
+            src_ref=src, dst_ref=dst, send_sem=ssem, recv_sem=rsem,
+            device_id=device, device_id_type=MESH,
+        )
+
+    barrier = pltpu.get_barrier_semaphore()
+    for k in range(1, 8):
+        pl.semaphore_signal(barrier, inc=1, device_id=ep_id(lax.rem(p + k, 8)), device_id_type=MESH)
+    pl.semaphore_signal(barrier, inc=1, device_id=core_id, device_id_type=MESH)
+    pl.semaphore_signal(barrier, inc=1, device_id=tp_id, device_id_type=MESH)
+
+    qc, kcs = wq_h.shape[1], wk_h.shape[1]
+    eff = eg_h.shape[2]
+    early = [
+        (tokens_h, tok),
+        (wq_h, w_qkv.at[c, :, pl.ds(0, qc)]),
+        (wk_h, w_qkv.at[c, :, pl.ds(qc, kcs)]),
+        (wv_h, w_qkv.at[c, :, pl.ds(qc + kcs, kcs)]),
+        (offset_h, off),
+        (lengths_h, lens),
+        (routes_h, routes),
+        (router_h, rt.at[0]),
+        (router_h, rt.at[1]),
+        (wo_h, w_o.at[c]),
+        (keys_h, kc),
+        (values_h, vc),
+        (sg_h, s1.at[:, pl.ds(0, eff)]),
+        (su_h, s1.at[:, pl.ds(eff, eff)]),
+        (sd_h, s2),
+        (eg_h.at[0], e1.at[c, :, pl.ds(0, eff)]),
+        (eu_h.at[0], e1.at[c, :, pl.ds(eff, eff)]),
+        (ed_h.at[0], e2.at[c]),
+    ]
+    local = [pltpu.make_async_copy(a, b, loc.at[i]) for i, (a, b) in enumerate(early)]
+    for copy in local:
+        copy.start()
+
+    local[0].wait()
+    data = tok[...].astype(F32)
+    factor = lax.rsqrt(jnp.mean(data * data, axis=-1, keepdims=True) + epsilon)
+    normed = (data * factor * gains_v[:, 0:width]).astype(BF16)
+    for k in range(8):
+        nrm[k] = normed[:, k * pair : (k + 1) * pair]
+
+    pl.semaphore_wait(barrier, 9)
+
+    def spread(src_at, dst, ssem, rsem):
+        out = []
+        for k in range(1, 8):
+            peer = lax.rem(p + k, 8)
+            out.append(remote(src_at(peer), dst.at[p], ssem.at[k], rsem.at[k], ep_id(peer)))
+        return out
+
+    def landing(src, dst, ssem, rsem):
+        out = []
+        for k in range(1, 8):
+            out.append(remote(src, dst.at[lax.rem(p - k + 8, 8)], ssem.at[k], rsem.at[k], ep_id(lax.rem(p + k, 8))))
+        return out
+
+    tok_copies = spread(lambda peer: nrm.at[peer], tok_in, tok_s, tok_r)
+    for copy in tok_copies:
+        copy.start()
+    pieces = [
+        (wq_h, w_qkv.at[c, :, pl.ds(0, qc)], w_qkv.at[1 - c, :, pl.ds(0, qc)]),
+        (wk_h, w_qkv.at[c, :, pl.ds(qc, kcs)], w_qkv.at[1 - c, :, pl.ds(qc, kcs)]),
+        (wv_h, w_qkv.at[c, :, pl.ds(qc + kcs, kcs)], w_qkv.at[1 - c, :, pl.ds(qc + kcs, kcs)]),
+        (wo_h, w_o.at[c], w_o.at[1 - c]),
+        (eg_h.at[0], e1.at[c, :, pl.ds(0, eff)], e1.at[1 - c, :, pl.ds(0, eff)]),
+        (eu_h.at[0], e1.at[c, :, pl.ds(eff, eff)], e1.at[1 - c, :, pl.ds(eff, eff)]),
+        (ed_h.at[0], e2.at[c], e2.at[1 - c]),
+    ]
+    core_out = [remote(a, b, core_s.at[i], core_r.at[i], core_id) for i, (a, b, _) in enumerate(pieces)]
+    core_in = [remote(a, d, core_s.at[i], core_r.at[i], core_id) for i, (a, _, d) in enumerate(pieces)]
+    for copy in core_out:
+        copy.start()
+    tok_in[p] = nrm[p]
+
+    ri = lax.broadcasted_iota(jnp.int32, (256, 256), 0)
+    ci = lax.broadcasted_iota(jnp.int32, (256, 256), 1)
+    perm = (ci == 2 * lax.rem(ri, 128) + ri // 128).astype(F32).astype(BF16)
+    same = lax.rem(ri, 2) == lax.rem(ci, 2)
+    ones[:, 0:256] = jnp.where(same & (ri > ci), 1.0, 0.0).astype(BF16)
+    ones[:, 256:512] = jnp.where(same, 1.0, 0.0).astype(BF16)
+
+    def split(values):
+        high = values.astype(BF16)
+        return high, (values - high.astype(F32)).astype(BF16)
+
+    local[4].wait()
+    local[5].wait()
+    for m in range(span // 256):
+        cols = pl.ds(m * 128, 128)
+        left = jnp.concatenate([off[:, 0, cols], off[:, 1, cols]], axis=0)
+        right = jnp.concatenate([off[:, 2, cols], off[:, 3, cols]], axis=0)
+        high, low = split(jnp.concatenate([left, right], axis=1))
+        oint[:, m * 256 : (m + 1) * 256] = jnp.dot(high, perm, preferred_element_type=F32) + jnp.dot(
+            low, perm, preferred_element_type=F32
+        )
+    rows2 = 2 * seqs
+    lane_id = lax.broadcasted_iota(jnp.int32, (rows2, seqs), 1)
+    row_id = lax.rem(lax.broadcasted_iota(jnp.int32, (rows2, seqs), 0), seqs)
+    limit = jnp.sum(
+        jnp.where(lane_id == row_id, jnp.broadcast_to(lens[...].astype(F32), (rows2, seqs)), 0.0),
+        axis=1, keepdims=True,
+    )
+
+    for i in (1, 2, 3):
+        local[i].wait()
+    for i in range(3):
+        core_in[i].wait_recv()
+    for copy in landing(nrm.at[0], tok_in, tok_s, tok_r):
+        copy.wait_recv()
+    feats = tok_in[...].reshape(8 * seqs, pair)
+    qw = w_qkv[:, :, 0:qc].reshape(pair, qc)
+    q_send[...] = jnp.dot(feats, qw, preferred_element_type=F32).astype(BF16).reshape(8, seqs, qc)
+    q_copies = spread(lambda peer: q_send.at[peer], q_in, qs, qr)
+    for copy in q_copies:
+        copy.start()
+    q_in[p] = q_send[p]
+    kvw = w_qkv[:, :, qc:].reshape(pair, 2 * kcs)
+    kv_send[...] = jnp.dot(feats, kvw, preferred_element_type=F32).astype(BF16).reshape(8, seqs, 2 * kcs)
+    kv_in[p] = kv_send[p]
+    local[10].wait()
+    local[11].wait()
+    for copy in landing(q_send.at[0], q_in, qs, qr):
+        copy.wait_recv()
+    kv_copies = spread(lambda peer: kv_send.at[peer], kv_in, kvs, kvr)
+    for copy in kv_copies:
+        copy.start()
+
+    queries = jnp.sum(q_in[...].astype(F32), axis=0)
+    for r in range(4):
+        q4[:, r, :] = queries[:, r * 128 : (r + 1) * 128]
+    even_row = lax.rem(lax.broadcasted_iota(jnp.int32, (1, span), 1), 2) == 0
+
+    def score(b, _):
+        s = lax.dot_general(
+            q4[b].astype(BF16), kc[b], (((1,), (1,)), ((), ())), preferred_element_type=F32
+        )
+        tmat[pl.ds(b, 1), :] = jnp.where(even_row, s[0:1], s[2:3])
+        tmat[pl.ds(seqs + b, 1), :] = jnp.where(even_row, s[1:2], s[3:4])
+        return 0
+
+    lax.fori_loop(0, seqs, score, 0, unroll=2)
+
+    blocks = span // 256
+    scale = 128.0 ** (-0.5)
+    lane = lax.broadcasted_iota(jnp.int32, (rows2, 256), 1)
+    even = lax.rem(lane, 2) == 0
+    place = (lane // 2).astype(F32)
+    for m in range(blocks):
+        cols = slice(m * 256, (m + 1) * 256)
+        part = slice(m * rows2, (m + 1) * rows2)
+        logits = tmat[:, cols] * scale + oint[:, cols]
+        log_sig = jnp.minimum(logits, 0.0) - jnp.log(1.0 + jnp.exp(-jnp.abs(logits)))
+        keep = jnp.where(place < limit - (m * 128), log_sig - logits, 0.0)
+        high, low = split(keep)
+        tmat[:, cols] = log_sig
+        hilo[0, part] = high
+        hilo[1, part] = low
+    sums[...] = jnp.dot(
+        hilo[...].reshape(2 * blocks * rows2, 256), ones[...], preferred_element_type=F32
+    ).reshape(2, blocks * rows2, 512)
+    carry = jnp.zeros((rows2, 256), F32)
+    for m in range(blocks - 1, -1, -1):
+        cols = slice(m * 256, (m + 1) * 256)
+        part = slice(m * rows2, (m + 1) * rows2)
+        after = carry + (sums[0, part, 0:256] + sums[1, part, 0:256])
+        carry = carry + (sums[0, part, 256:512] + sums[1, part, 256:512])
+        sticks = jnp.where(place < limit - (m * 128), jnp.exp(tmat[:, cols] + after), 0.0)
+        on_even = jnp.where(even, sticks, 0.0)
+        on_odd = jnp.where(even, 0.0, sticks)
+        p4[:, 0, cols] = on_even[0:seqs]
+        p4[:, 1, cols] = on_even[seqs:]
+        p4[:, 2, cols] = on_odd[0:seqs]
+        p4[:, 3, cols] = on_odd[seqs:]
+
+    def weigh(b, _):
+        ho[b] = jnp.dot(p4[b].astype(BF16), vc[b], preferred_element_type=F32)
+        return 0
+
+    lax.fori_loop(0, seqs, weigh, 0, unroll=2)
+    heads = jnp.concatenate([ho[:, r, :] for r in range(4)], axis=1)
+    scaled = (heads * gains_v[:, 2 * width : 2 * width + qc]).astype(BF16)
+    sc_in[p] = scaled
+    square = jnp.broadcast_to(jnp.sum(heads * heads, axis=-1, keepdims=True), (seqs, 128))
+    sq_send[...] = square
+    sc_copies = spread(lambda peer: sc_in.at[p], sc_in, scs, scr)
+    for copy in sc_copies:
+        copy.start()
+    sq_copy = remote(sq_send, sq_in, sqs.at[0], sqr.at[0], tp_id)
+    sq_copy.start()
+
+    local[9].wait()
+    core_in[3].wait_recv()
+    for copy in landing(sc_in.at[p], sc_in, scs, scr):
+        copy.wait_recv()
+    f_send[...] = lax.dot_general(
+        sc_in[...].reshape(8 * seqs, qc), w_o[...].reshape(pair, qc), (((1,), (1,)), ((), ())),
+        preferred_element_type=F32,
+    ).astype(BF16).reshape(8, seqs, pair)
+    f_copies = spread(lambda peer: f_send.at[peer], f_in, fs, fr)
+    for copy in f_copies:
+        copy.start()
+    f_in[p] = f_send[p]
+    g_copies = [remote(f_in.at[p], f_in2.at[p], gs.at[0], gr.at[0], tp_id)]
+    g_copies[0].start()
+    f_land = landing(f_send.at[0], f_in, fs, fr)
+    for k in range(1, 8):
+        f_land[k - 1].wait_recv()
+        slot = lax.rem(p - k + 8, 8)
+        copy = remote(f_in.at[slot], f_in2.at[slot], gs.at[k], gr.at[k], tp_id)
+        copy.start()
+        g_copies.append(copy)
+    sq_copy.wait_recv()
+    for copy in g_copies:
+        copy.wait_recv()
+    total = sq_send[:, 0:1] + sq_in[:, 0:1]
+    norm = lax.rsqrt(total / (HQ * HD) + epsilon)
+    attention = jnp.concatenate([f_in[k].astype(F32) + f_in2[k].astype(F32) for k in range(8)], axis=1) * norm
+    residual = (tok[...].astype(F32) + attention).astype(BF16).astype(F32)
+    resid[0] = residual[:, 0:half]
+    resid[1] = residual[:, half:]
+    factor = lax.rsqrt(jnp.mean(residual * residual, axis=-1, keepdims=True) + epsilon)
+    nf = (residual * factor * gains_v[:, width : 2 * width]).astype(BF16)
+
+    for i in (6, 7, 8):
+        local[i].wait()
+    router = jnp.concatenate([rt[0], rt[1]], axis=0)
+    pads = 128 - 2 * experts
+    router = jnp.concatenate([router, jnp.zeros((pads, width), BF16)], axis=0)
+    prob = jax.nn.sigmoid(
+        lax.dot_general(nf, router, (((1,), (1,)), ((), ())), preferred_element_type=F32)
+    )
+    sub = lax.broadcasted_iota(jnp.int32, (128, seqs), 0)
+    sub = jnp.where(sub < 2 * experts, lax.rem(sub, experts), -1)
+    named = jnp.zeros((128, seqs), F32)
+    for k in range(routes.shape[0]):
+        named = named + jnp.where(sub == routes[k : k + 1, :], 1.0, 0.0)
+    eye = jnp.where(
+        lax.broadcasted_iota(jnp.int32, (seqs, seqs), 0) == lax.broadcasted_iota(jnp.int32, (seqs, seqs), 1), 1.0, 0.0
+    ).astype(BF16)
+    hot = lax.dot_general(eye, named.astype(BF16), (((1,), (1,)), ((), ())), preferred_element_type=F32)
+    picked = hot * prob
+    lanes = lax.broadcasted_iota(jnp.int32, (seqs, 128), 1)
+    bottom = jnp.sum(jnp.where(lanes < experts, picked, 0.0), axis=-1, keepdims=True)
+    share = routed_scale * picked / bottom
+    high, low = split(share)
+    nf_in[p, :, 0:width] = nf
+    nf_in[p, :, width : width + 128] = jnp.where(lanes < experts, high.astype(F32), low.astype(F32)).astype(BF16)
+
+    xp = z * 2 + (1 - x)
+    nx_copies = [remote(nf_in.at[p], nf_in.at[p], nxs.at[0], nxr.at[0], ep_id(xp))]
+    nz_copies = []
+    for k in range(1, 4):
+        peer = lax.rem(z + k, 4) * 2 + x
+        nz_copies.append(remote(nf_in.at[p], nf_in.at[p], nzs.at[k], nzr.at[k], ep_id(peer)))
+    for copy in nz_copies:
+        copy.start()
+    nx_copies[0].start()
+
+    for i in (12, 13, 14):
+        local[i].wait()
+    gu = jnp.dot(nf, s1[...], preferred_element_type=F32)
+    hidden = (jax.nn.silu(gu[:, 0:eff]) * gu[:, eff:]).astype(BF16)
+    shared = jnp.dot(hidden, s2[...], preferred_element_type=F32)
+
+    for k in range(1, 4):
+        slot = lax.rem(z - k + 4, 4) * 2 + x
+        remote(nf_in.at[p], nf_in.at[slot], nzs.at[k], nzr.at[k], ep_id(p)).wait_recv()
+        copy = remote(nf_in.at[slot], nf_in.at[slot], nxs.at[k], nxr.at[k], ep_id(xp))
+        copy.start()
+        nx_copies.append(copy)
+    for i in (15, 16, 17):
+        local[i].wait()
+    for i in (4, 5, 6):
+        core_in[i].wait_recv()
+    for k in range(4):
+        slot = lax.rem(z - k + 4, 4) * 2 + (1 - x)
+        remote(nf_in.at[p], nf_in.at[slot], nxs.at[k], nxr.at[k], ep_id(xp)).wait_recv()
+
+    everyone = nf_in[:, :, 0:width].reshape(8 * seqs, width)
+    shares = nf_in[:, :, width : width + 128].reshape(8 * seqs, 128).astype(F32)
+    big_lane = lax.broadcasted_iota(jnp.int32, (8 * seqs, 128), 1)
+    routed = []
+    for j in range(2):
+        mine = 2 * p + j
+        col = jnp.sum(
+            jnp.where((big_lane == mine) | (big_lane == experts + mine), shares, 0.0), axis=-1, keepdims=True
+        )
+        gu = jnp.dot(everyone, e1[j], preferred_element_type=F32)
+        routed.append((jax.nn.silu(gu[:, 0:eff]) * gu[:, eff:] * col).astype(BF16))
+    acts = jnp.concatenate(routed, axis=1)
+    for g in range(4):
+        cols = slice(g * (width // 4), (g + 1) * (width // 4))
+        part = jnp.dot(acts, e2[:, :, cols].reshape(2 * eff, width // 4), preferred_element_type=F32)
+        inner = slice((g % 2) * (half // 2), (g % 2 + 1) * (half // 2))
+        d_send[g // 2, :, :, inner] = part.astype(BF16).reshape(8, seqs, width // 4)
+    d_send[0, p] = (d_send[0, p].astype(F32) + shared[:, 0:half]).astype(BF16)
+    d_send[1, p] = (d_send[1, p].astype(F32) + shared[:, half:]).astype(BF16)
+
+    y_copies = {}
+    for side in (1, 0):
+        for k in (1, 2, 3, 0):
+            xx = lax.rem(x + side, 2)
+            slot = lax.rem(z + k, 4) * 2 + xx
+            yslot = lax.rem(z + k, 4) * 2 + xx
+            copy = remote(d_send.at[1 - t, slot], y_in.at[yslot], ys.at[4 * side + k], yr.at[4 * side + k], tp_id)
+            copy.start()
+            y_copies[side, k] = copy
+    x_copies = {}
+    for k in (1, 2, 3, 0):
+        slot = lax.rem(z + k, 4) * 2 + (1 - x)
+        y_copies[1, k].wait_recv()
+        x_send[k] = (d_send[t, slot].astype(F32) + y_in[slot].astype(F32)).astype(BF16)
+        copy = remote(x_send.at[k], x_in.at[k], xs.at[k], xr.at[k], ep_id(xp))
+        copy.start()
+        x_copies[k] = copy
+    z_copies = {}
+    for k in (1, 2, 3, 0):
+        zz = lax.rem(z + k, 4)
+        slot = zz * 2 + x
+        y_copies[0, k].wait_recv()
+        x_copies[k].wait_recv()
+        summed = d_send[t, slot].astype(F32) + y_in[slot].astype(F32) + x_in[k].astype(F32)
+        if k > 0:
+            z_send[k - 1] = summed.astype(BF16)
+            copy = remote(z_send.at[k - 1], z_in.at[k - 1], zs.at[k], zr.at[k], ep_id(slot))
+            copy.start()
+            z_copies[k] = copy
+    for copy in landing(kv_send.at[0], kv_in, kvs, kvr):
+        copy.wait_recv()
+    fresh = jnp.sum(kv_in[...].astype(F32), axis=0)
+    fk_o[...] = fresh[:, 0:kcs].astype(BF16)
+    fv_o[...] = fresh[:, kcs:].astype(BF16)
+    for k in range(1, 4):
+        z_copies[k].wait_recv()
+        summed = summed + z_in[k - 1].astype(F32)
+    mixed_o[...] = (resid[t] + summed).astype(BF16)
+
+    for copy in (
+        tok_copies + core_out + q_copies + kv_copies + sc_copies + [sq_copy] + f_copies + g_copies
+        + nz_copies + nx_copies + list(y_copies.values()) + list(x_copies.values()) + list(z_copies.values())
+    ):
+        copy.wait_send()
+
+
+def fused_body(
+    ep_count, tp_count, tokens, attn_gain, query_weight, key_weight, value_weight, out_weight, head_gain,
+    past_keys, past_values, break_offset, cache_lengths, ffn_gain, router_weight, expert_routes,
+    expert_gate, expert_up, expert_down, shared_gate, shared_up, shared_down,
+):
+    seqs, width = tokens.shape
+    pair = width // 8
+    half = width // 2
+    rows, qc = query_weight.shape
+    kcs = key_weight.shape[1]
+    positions = past_keys.shape[1]
+    span = 2 * positions
+    eff = expert_gate.shape[2]
+    experts = router_weight.shape[1]
+    tops = expert_routes.shape[1]
+    gains = jnp.concatenate([attn_gain, ffn_gain, head_gain]).astype(F32)[None, :]
+    operands = (
+        tokens, gains, query_weight, key_weight, value_weight, out_weight,
+        past_keys.reshape(seqs, span, HD), past_values.reshape(seqs, span, HD),
+        break_offset, cache_lengths.reshape(1, seqs), router_weight.T, expert_routes.T,
+        expert_gate, expert_up, expert_down, shared_gate, shared_up, shared_down,
+    )
+    anywhere = pl.BlockSpec(memory_space=pl.ANY)
+    inside = pl.BlockSpec(memory_space=pltpu.VMEM)
+    vm = pltpu.VMEM
+    dma = pltpu.SemaphoreType.DMA
+    scratch = [
+        vm((seqs, width), BF16), vm((2, rows, qc + 2 * kcs), BF16), vm((2, rows, qc), BF16),
+        vm((seqs, span, HD), BF16), vm((seqs, span, HD), BF16), vm(break_offset.shape, F32),
+        vm((1, seqs), jnp.int32), vm((2, experts, width), BF16), vm((tops, seqs), jnp.int32),
+        vm((2, width, 2 * eff), BF16), vm((2, eff, width), BF16), vm((width, 2 * eff), BF16), vm((eff, width), BF16),
+        vm((8, seqs, pair), BF16), vm((8, seqs, pair), BF16),
+        vm((8, seqs, qc), BF16), vm((8, seqs, qc), BF16), vm((8, seqs, 2 * kcs), BF16), vm((8, seqs, 2 * kcs), BF16),
+        vm((seqs, 4, HD), F32), vm((2 * seqs, span), F32), vm((2 * seqs, span), F32), vm((seqs, 4, span), F32),
+        vm((seqs, 4, HD), F32),
+        vm((8, seqs, qc), BF16), vm((8, seqs, pair), BF16), vm((8, seqs, pair), BF16), vm((8, seqs, pair), BF16),
+        vm((seqs, 128), F32), vm((seqs, 128), F32), vm((8, seqs, width + 128), BF16), vm((2, seqs, half), F32),
+        vm((2, 8, seqs, half), BF16), vm((8, seqs, half), BF16), vm((4, seqs, half), BF16), vm((4, seqs, half), BF16),
+        vm((3, seqs, half), BF16), vm((3, seqs, half), BF16),
+        vm((2, span // 256 * 2 * seqs, 256), BF16), vm((256, 512), BF16), vm((2, span // 256 * 2 * seqs, 512), F32),
+        dma((18,)), dma((7,)), dma((7,)),
+        dma((8,)), dma((8,)), dma((8,)), dma((8,)), dma((8,)), dma((8,)), dma((8,)), dma((8,)),
+        dma((8,)), dma((8,)), dma((8,)), dma((8,)), dma((1,)), dma((1,)),
+        dma((4,)), dma((4,)), dma((4,)), dma((4,)), dma((8,)), dma((8,)), dma((4,)), dma((4,)), dma((4,)), dma((4,)),
+    ]
+    return pl.pallas_call(
+        fused_kernel,
+        out_shape=(
+            jax.ShapeDtypeStruct((seqs, half), BF16),
+            jax.ShapeDtypeStruct((seqs, kcs), BF16),
+            jax.ShapeDtypeStruct((seqs, kcs), BF16),
+        ),
+        in_specs=[inside if i == 1 else anywhere for i in range(len(operands))],
+        out_specs=(inside, inside, inside),
+        scratch_shapes=scratch,
+        compiler_params=pltpu.CompilerParams(
+            collective_id=0, has_side_effects=True, vmem_limit_bytes=60 * 1024 * 1024
+        ),
+    )(*operands)
+
+
 def solution(mesh):
     placed = (
         P("ep", None),
@@ -179,8 +642,15 @@
         P(None, "tp"),
         P("tp", None),
     )
+    ep_count, tp_count = mesh.shape["ep"], mesh.shape["tp"]
+
+    def chosen_body(*arrays):
+        if fits(ep_count, tp_count, arrays):
+            return fused_body(ep_count, tp_count, *arrays)
+        return body(*arrays)
+
     return jax.shard_map(
-        body,
+        chosen_body,
         mesh=mesh,
         in_specs=placed,
         out_specs=(P("ep", "tp"), P("ep", "tp"), P("ep", "tp")),

time: 281 us -> 65.7 us (0.23)
  waiting for transfers between devices: 86.1 us -> 0 us
  Pallas kernels: 0 us -> 58 us
  other arithmetic: 47.6 us -> 0.63 us
  blocking collectives: 44.1 us -> 0 us
  local copies, waits for them, and re-layouts: 41.1 us -> 6.03 us
  matrix products: 25.1 us -> 0 us
  starting transfers between devices: 21.5 us -> 0 us
  between operations: 14.4 us -> 0.64 us
    pallas_call x0 -> x1, Pallas kernels: none -> 58 us  [fused_body(): pl.pallas_call(fused_kernel, out_shape=(jax.ShapeDtypeStruct((seqs, half)...]
    reduce_scatter x1 -> x0, waiting for transfers between devices: 50.7 us -> none  [body(): lax.psum_scatter(jnp.dot(features, joined, preferred_element_type=jnp.flo...]
    all_to_all x5 -> x0, waiting for transfers between devices: 35.4 us -> none  [the longest x1 21.8 us: body(): lax.all_to_all(outbound, 'ep', split_axis=0, concat_axis=0, tiled=True)]
    all_gather x2 -> x0, blocking collectives: 25.1 us -> none  [the longest x1 20.1 us: body(): lax.all_gather(scaled, 'ep', axis=0, tiled=True)]
    dot_general x13 -> x0, matrix products: 25.1 us -> none  [the longest x1 5.64 us: stick_attend(): jnp.einsum('bgrd,blgd->bgrl', grouped, key_cache, preferred_element_type=...]
    all_to_all x5 -> x0, starting transfers between devices: 21.4 us -> none  [the longest x1 6.84 us: body(): lax.all_to_all(expert_total.astype(jnp.bfloat16), 'ep', split_axis=0, con...]
    another operation x5 -> x0, other arithmetic: 19.2 us -> none
    unnamed x18 -> x3, local copies, waits for them, and re-layouts: 22.6 us -> 3.96 us
  transfers between devices with their start and end apart: 6 -> 0, of which waited for: 4 -> 0; matrix products, arithmetic and copies ran while one was open for 18% -> 0% of each run, Pallas kernels for 0% -> 0%
where the time goes in v1:
time: 65.7 us; the launch traced here: 65.3 us
  Pallas kernels  58 us (88%)
  local copies, waits for them, and re-layouts  6.03 us (9%)
    pallas_call x1, Pallas kernels, fused_body(): pl.pallas_call(fused_kernel, out_shape=(jax.ShapeDtypeStruct((seqs, half)...  58 us
    unnamed x3, local copies, waits for them, and re-layouts  3.96 us
    concatenate x3, local copies, waits for them, and re-layouts, fused_body(): jnp.concatenate([attn_gain, ffn_gain, head_gain]).astype(F32)[None, :]  2.07 us

profile of v1, /device:TPU:0, one launch (start us, length us, event | category | flops | bytes accessed | tf_op | source)
XLA Modules:
  0.0 65.3 jit_solution(3077206353331727737)
XLA Ops:
  0.6 0.7 %concatenate.18 = bf16[1,512]{1,0:T(2,128)(2,1)S(1)} reshape(bf16[512]{0:T(512)(128)(2,1)} %param.26) | data formatting | bytes 2048 | tf_op jit(solution)/shard_map/concatenate | solution.py:576
  1.3 0.7 %concatenate.16 = bf16[1,2048]{1,0:T(2,128)(2,1)S(1)} reshape(bf16[2048]{0:T(1024)(128)(2,1)} %param.21) | data formatting | bytes 8192 | tf_op jit(solution)/shard_map/concatenate | solution.py:576
  2.0 0.7 %concatenate.17 = bf16[1,2048]{1,0:T(2,128)(2,1)S(1)} reshape(bf16[2048]{0:T(1024)(128)(2,1)} %param.31) | data formatting | bytes 8192 | tf_op jit(solution)/shard_map/concatenate | solution.py:576
  2.7 0.6 maximum_convert_fusion.gains_v
  3.3 58.0 %shard_map.211 = (bf16[16,1024]{1,0:T(8,128)(2,1)}, bf16[16,256]{1,0:T(8,128)(2,1)}, bf16[16,256]{1,0:T(8,128)(2,1)}) custom-call(bf16[16,2048]{1,0:T(8,128)(2,1)} %tokens_h.1, f32[1,4608]{1,0:T(1,128)} %maximum_convert_fusion.gains_v, bf16[128,512]{1,0:T(8,128)(2,1)} %wq_h.1, bf16[128,256]{1,0:T(8,128)(2,1)} %wk_h.1, bf16[128,256]{1,0:T(8,128)(2,1)} %wv_h.1, ...), custom_call_target="tpu_custom_call" | custom-call | tf_op jit(solution)/shard_map/pallas_call | solution.py:606
  61.3 1.4 %copy.26 = bf16[16,1024]{1,0:T(8,128)(2,1)} copy(bf16[16,1024]{1,0:T(8,128)(2,1)} %get-tuple-element.6) | data formatting | bytes 65536
  62.7 1.3 %copy.27 = bf16[16,256]{1,0:T(8,128)(2,1)} copy(bf16[16,256]{1,0:T(8,128)(2,1)} %get-tuple-element.7) | data formatting | bytes 16384
  64.0 1.3 %copy.28 = bf16[16,256]{1,0:T(8,128)(2,1)} copy(bf16[16,256]{1,0:T(8,128)(2,1)} %get-tuple-element.8) | data formatting | bytes 16384
